TPU v7x, 1024 devices: a whole 4x8x16 slice. The times are simulated.
1024 devices in a mesh: tp: 32 (over z, core), dp: 32 (over y, x).
Axes of the slice: x: 4, y: 8, z: 16, core: 2. Of those that a mesh axis runs over, the one named last changes fastest.
Arguments:
- tokens: bfloat16 [256, 4096], P('tp', 'dp'), may hold values from -30 to 30
- lengths: int32 [256], P('dp'), may hold values from 1 to 8192, 524288 in all
- in_gain: float32 [2, 4096], P(None, 'dp'), may hold values from 0.1 to 1.9
- w_recept: bfloat16 [2, 4096, 2048], P(None, 'dp', 'tp'), may hold values from -0.09375 to 0.09375
- w_key: bfloat16 [2, 4096, 2048], P(None, 'dp', 'tp'), may hold values from -0.09375 to 0.09375
- w_value: bfloat16 [2, 4096, 2048], P(None, 'dp', 'tp'), may hold values from -0.09375 to 0.09375
- w_decay: bfloat16 [2, 4096, 2048], P(None, 'dp', 'tp'), may hold values from -0.09375 to 0.09375
- w_rate: bfloat16 [2, 4096, 2048], P(None, 'dp', 'tp'), may hold values from -0.09375 to 0.09375
- w_gate: bfloat16 [2, 4096, 2048], P(None, 'dp', 'tp'), may hold values from -0.09375 to 0.09375
- w_out: bfloat16 [2, 2048, 4096], P(None, 'tp', 'dp'), may hold values from -0.125 to 0.125
- decay_base: float32 [2, 2048], P(None, 'tp'), may hold values from -6 to 6
- mix_gain: float32 [2, 2048], P(None, 'tp'), may hold values from 0.1 to 1.9
- states: float32 [2, 256, 32, 64, 64], P(None, 'dp', 'tp'), may hold values from -6 to 6
Outputs:
- next_tokens: bfloat16 [256, 4096], P('tp', 'dp')
- new_states: float32 [2, 256, 32, 64, 64], P(None, 'dp', 'tp')
All inputs are finite; a program needn't handle non-finite values. No bound on the sum of `lengths` on one device may be relied on, other than what follows from the above.
Results may differ from a plain program's by a relative error of at most 0.0065.
Values may be sent and summed in bfloat16 or wider, within the bound.
A program may use at most 32 MiB of HBM per device.

v0:
```python
import jax
import jax.numpy as jnp
from jax import lax
from jax.sharding import PartitionSpec as P

D = 4096
LAYERS = 2
POSITION = 2048


DECAY_SCALE = 0.6065306597126334
NORM_EPS = 1e-06
KEY_EPS = 1e-05
GROUP_EPS = 0.00064


def laid_out(pieces, dim):
    pieces = jnp.moveaxis(pieces, 0, dim)
    dims = pieces.shape
    return pieces.reshape(*dims[:dim], dims[dim] * dims[dim + 1], *dims[dim + 2 :])


def sent_to_all(array, axis):
    size = lax.axis_size(axis)
    return lax.all_to_all(
        jnp.broadcast_to(array[None], (size, *array.shape)), axis, 0, 0, tiled=True
    )


def gather_directly(array, axis, dim):
    return laid_out(sent_to_all(array, axis), dim)


def cut_along(array, dim, size):
    before, after = (array.shape[:dim], array.shape[dim + 1 :])
    return jnp.moveaxis(array.reshape(*before, size, -1, *after), dim, 0)


def sum_at_owner(array, axis, dim):
    size = lax.axis_size(axis)
    pieces = lax.all_to_all(cut_along(array, dim, size), axis, 0, 0, tiled=True)
    return jnp.sum(pieces, axis=0)


def sent_together(arrays, axis, dim, along):
    columns = [a.reshape(*a.shape[:along], -1) for a in arrays]
    both = jnp.concatenate(columns, axis=along)
    whole, at, gathered = (sum_at_owner(both, axis, dim), 0, [])
    for a, column in zip(arrays, columns):
        slab = whole[..., at : at + column.shape[along]]
        gathered.append(slab.reshape(*slab.shape[:along], *a.shape[along:]))
        at += column.shape[along]
    return tuple(gathered)


def update_heads(projected, previous, base_row, gain_row, alive_rows):
    row_count = previous.shape[0]
    head_count = previous.shape[1]
    head_size = previous.shape[2]
    local_width = head_count * head_size
    role_parts = [
        projected[:, role_index * local_width : (role_index + 1) * local_width]
        for role_index in range(6)
    ]
    recept, key_flat, value_flat, decay_pre, rate_pre, gate_pre = role_parts
    decay_factor = jnp.exp(-DECAY_SCALE * jax.nn.sigmoid(decay_pre + base_row))
    in_rate = jax.nn.sigmoid(rate_pre)
    key_heads = key_flat.reshape(row_count, head_count, head_size)
    unit_key = key_heads * lax.rsqrt(
        jnp.sum(key_heads * key_heads, axis=2, keepdims=True) + KEY_EPS
    )
    removed = jnp.einsum("bhvk,bhk->bhv", previous, -unit_key, precision=lax.Precision.HIGHEST)
    decay_heads = decay_factor.reshape(row_count, head_count, 1, head_size)
    rate_heads = in_rate.reshape(row_count, head_count, head_size)
    value_heads = value_flat.reshape(row_count, head_count, head_size)
    updated = (
        previous * decay_heads
        + removed[..., None] * (unit_key * rate_heads)[:, :, None, :]
        + value_heads[..., None] * key_heads[:, :, None, :]
    )
    recept_heads = recept.reshape(row_count, head_count, head_size)
    readout = jnp.einsum("bhvk,bhk->bhv", updated, recept_heads, precision=lax.Precision.HIGHEST)
    centre = jnp.mean(readout, axis=2, keepdims=True)
    spread = jnp.mean(jnp.square(readout - centre), axis=2, keepdims=True)
    normed = ((readout - centre) * lax.rsqrt(spread + GROUP_EPS)).reshape(row_count, local_width)
    normed = normed * gain_row * jax.nn.sigmoid(gate_pre)
    mixed_rows = jnp.where(alive_rows[:, None], normed, 0.0).astype(jnp.bfloat16)
    kept_state = jnp.where(alive_rows[:, None, None, None], updated, previous)
    return (mixed_rows, kept_state)


def on_device(
    tokens,
    lengths,
    in_gain,
    w_recept,
    w_key,
    w_value,
    w_decay,
    w_rate,
    w_gate,
    w_out,
    decay_base,
    mix_gain,
    states,
):
    dp_count = lax.axis_size("dp")
    shard_rows = states.shape[1]
    groups = 1
    portion_rows = shard_rows // groups
    alive_rows = lengths > POSITION
    current = tokens
    kept_states = []
    for layer_index in range(LAYERS):
        gathered = gather_directly(current, "tp", 0)
        widened = gathered.astype(jnp.float32)
        squares = jnp.sum(widened * widened, axis=1)
        scaled = (widened * in_gain[layer_index]).astype(jnp.bfloat16)
        joined = jnp.concatenate(
            [
                w_recept[layer_index],
                w_key[layer_index],
                w_value[layer_index],
                w_decay[layer_index],
                w_rate[layer_index],
                w_gate[layer_index],
            ],
            axis=1,
        )
        local_cols = scaled.shape[1]
        ordered = scaled.reshape(dp_count, groups, portion_rows, local_cols)
        ordered_squares = squares.reshape(dp_count, groups, portion_rows)
        portion = ordered[:, 0].reshape(dp_count * portion_rows, local_cols)
        partials = jnp.dot(portion, joined, preferred_element_type=jnp.float32)
        portion_sq = ordered_squares[:, 0].reshape(dp_count * portion_rows)
        summed, summed_squares = sent_together((partials, portion_sq), "dp", 0, 1)
        projected = summed
        inverse = lax.rsqrt(summed_squares / D + NORM_EPS)
        projected = projected * inverse[:, None]
        mixed_rows, kept_state = update_heads(
            projected,
            states[layer_index],
            decay_base[layer_index],
            mix_gain[layer_index],
            alive_rows,
        )
        out_weight = w_out[layer_index]

        def output_rows(block_part, offset, out_weight=out_weight):
            return jnp.dot(block_part, out_weight, preferred_element_type=jnp.float32)

        head_terms = output_rows(gather_directly(mixed_rows, "dp", 0), jnp.int32(0))
        branch = sum_at_owner(head_terms, "tp", 0)
        current = (current.astype(jnp.float32) + branch).astype(jnp.bfloat16)
        kept_states.append(kept_state)
    return (current, jnp.stack(kept_states))


def solution(mesh):
    in_specs = (
        P("tp", "dp"),
        P("dp"),
        P(None, "dp"),
        P(None, "dp", "tp"),
        P(None, "dp", "tp"),
        P(None, "dp", "tp"),
        P(None, "dp", "tp"),
        P(None, "dp", "tp"),
        P(None, "dp", "tp"),
        P(None, "tp", "dp"),
        P(None, "tp"),
        P(None, "tp"),
        P(None, "dp", "tp", None, None),
    )
    out_specs = (P("tp", "dp"), P(None, "dp", "tp", None, None))
    return jax.shard_map(
        on_device, mesh=mesh, in_specs=in_specs, out_specs=out_specs, check_vma=False
    )
```

profile of v0, /device:TPU:1, one launch (start us, length us, event | category | flops | bytes accessed | tf_op | source)
XLA Modules:
  0.0 182.1 jit_solution(7562530147818061830)
XLA Ops:
  0.6 1.3 broadcast_in_dim.36
  2.0 20.5 %all-to-all-start = ((bf16[32,8,128]{2,1,0:T(8,128)(2,1)}), bf16[32,8,128]{2,1,0:T(8,128)(2,1)S(1)}, u32[]{:S(2)}, u32[]{:S(2)}) async-start(bf16[32,8,128]{2,1,0:T(8,128)(2,1)} %broadcast_in_dim.36), calls=%async_computation | async-start | bytes 131072 | tf_op jit(solution)/shard_map/all_to_all | solution.py:25
  22.5 0.7 copy-done.2
  23.3 0.8 copy-done.3
  24.0 0.8 copy-done.4
  24.8 0.8 copy-done.5
  25.6 0.8 copy-done.6
  27.2 0.5 copy-done.9
  27.7 7.8 %all-to-all-done = bf16[32,8,128]{2,1,0:T(8,128)(2,1)S(1)} async-done(((bf16[32,8,128]{2,1,0:T(8,128)(2,1)}), bf16[32,8,128]{2,1,0:T(8,128)(2,1)S(1)}, u32[]{:S(2)}, u32[]{:S(2)}) %all-to-all-start) | async-done | bytes 65568 | tf_op jit(solution)/shard_map/all_to_all | solution.py:25
  35.6 0.3 copy.100
  36.1 0.9 pad_maximum_fusion
  36.9 9.8 %all-to-all-start.1 = ((f32[32,8,385]{2,1,0:T(8,128)}), f32[32,8,385]{2,1,0:T(8,128)S(1)}, u32[]{:S(2)}, u32[]{:S(2)}) async-start(f32[32,8,385]{2,1,0:T(8,128)} %pad_maximum_fusion), calls=%async_computation.1 | async-start | bytes 1048576 | tf_op jit(solution)/shard_map/all_to_all | solution.py:41
  46.8 15.1 %all-to-all-done.1 = f32[32,8,385]{2,1,0:T(8,128)S(1)} async-done(((f32[32,8,385]{2,1,0:T(8,128)}), f32[32,8,385]{2,1,0:T(8,128)S(1)}, u32[]{:S(2)}, u32[]{:S(2)}) %all-to-all-start.1) | async-done | bytes 394272 | tf_op jit(solution)/shard_map/all_to_all | solution.py:41
  62.4 0.5 fusion.6
  63.0 0.7 fusion.10
  64.2 14.8 %all_to_all.40 = bf16[32,2,256]{2,1,0:T(2,128)(2,1)S(1)} all-to-all(bf16[32,2,256]{2,1,0:T(2,128)(2,1)S(1)} %reshape.242), channel_id=1, replica_groups=mesh['tp'=32,'dp'=32] {'dp'}, dimensions={0} | all-to-all | bytes 65536 | tf_op jit(solution)/shard_map/all_to_all | solution.py:25
  79.1 0.6 copy-done.7
  79.9 22.7 %all_to_all.41 = f32[32,8,128]{2,1,0:T(8,128)S(1)} all-to-all(f32[32,8,128]{2,1,0:T(8,128)S(1)} %fusion.44), channel_id=1, replica_groups=mesh['tp'=32,'dp'=32] {'tp'}, dimensions={0} | all-to-all | bytes 262144 | tf_op jit(solution)/shard_map/all_to_all | solution.py:41
  102.6 0.6 copy-done.8
  103.3 0.6 broadcast_in_dim.39
  103.9 5.1 %all-to-all-start.4 = ((bf16[32,8,128]{2,1,0:T(8,128)(2,1)}), bf16[32,8,128]{2,1,0:T(8,128)(2,1)S(1)}, u32[]{:S(2)}, u32[]{:S(2)}) async-start(bf16[32,8,128]{2,1,0:T(8,128)(2,1)} %broadcast_in_dim.39), calls=%async_computation.4 | async-start | bytes 131072 | tf_op jit(solution)/shard_map/all_to_all | solution.py:25
  109.9 12.1 %all-to-all-done.4 = bf16[32,8,128]{2,1,0:T(8,128)(2,1)S(1)} async-done(((bf16[32,8,128]{2,1,0:T(8,128)(2,1)}), bf16[32,8,128]{2,1,0:T(8,128)(2,1)S(1)}, u32[]{:S(2)}, u32[]{:S(2)}) %all-to-all-start.4) | async-done | bytes 65568 | tf_op jit(solution)/shard_map/all_to_all | solution.py:25
  122.7 18.3 %all_to_all.42 = f32[32,8,385]{2,1,0:T(8,128)S(1)} all-to-all(f32[32,8,385]{2,1,0:T(8,128)S(1)} %pad_maximum_fusion.1), channel_id=1, replica_groups=mesh['tp'=32,'dp'=32] {'dp'}, dimensions={0} | all-to-all | bytes 788480 | tf_op jit(solution)/shard_map/all_to_all | solution.py:41
  141.5 0.5 fusion
  142.0 0.7 fusion.4
  143.3 14.6 %all_to_all.43 = bf16[32,2,256]{2,1,0:T(2,128)(2,1)S(1)} all-to-all(bf16[32,2,256]{2,1,0:T(2,128)(2,1)S(1)} %reshape.244), channel_id=1, replica_groups=mesh['tp'=32,'dp'=32] {'dp'}, dimensions={0} | all-to-all | bytes 65536 | tf_op jit(solution)/shard_map/all_to_all | solution.py:25
  158.0 0.8 fusion.42
  158.7 6.6 %all-to-all-start.7 = ((f32[32,8,128]{2,1,0:T(8,128)}), f32[32,8,128]{2,1,0:T(8,128)S(1)}, u32[]{:S(2)}, u32[]{:S(2)}) async-start(f32[32,8,128]{2,1,0:T(8,128)} %fusion.42), calls=%async_computation.7 | async-start | bytes 262144 | tf_op jit(solution)/shard_map/all_to_all | solution.py:41
  165.3 0.4 add_select_fusion.1
  165.7 0.8 pad_maximum_fusion.2
  166.5 15.0 %all-to-all-done.7 = f32[32,8,128]{2,1,0:T(8,128)S(1)} async-done(((f32[32,8,128]{2,1,0:T(8,128)}), f32[32,8,128]{2,1,0:T(8,128)S(1)}, u32[]{:S(2)}, u32[]{:S(2)}) %all-to-all-start.7) | async-done | bytes 131104 | tf_op jit(solution)/shard_map/all_to_all | solution.py:41
  181.5 0.6 add_convert_fusion
  (80 shorter events, 5.2 us)
Async XLA Ops:
  1.9 20.5 %copy-start.1 = (bf16[2,128,64]{1,2,0:T(8,128)(2,1)S(1)}, bf16[2,128,64]{1,2,0:T(8,128)(2,1)}, u32[]{:S(2)}) copy-start(bf16[2,128,64]{1,2,0:T(8,128)(2,1)} %param.16) | copy-start | bytes 98308
  2.0 33.6 %all-to-all-start = ((bf16[32,8,128]{2,1,0:T(8,128)(2,1)}), bf16[32,8,128]{2,1,0:T(8,128)(2,1)S(1)}, u32[]{:S(2)}, u32[]{:S(2)}) async-start(bf16[32,8,128]{2,1,0:T(8,128)(2,1)} %broadcast_in_dim.36), calls=%async_computation | async-start | bytes 131072 | tf_op jit(solution)/shard_map/all_to_all | solution.py:25
  22.5 0.8 copy-start.2
  23.3 0.8 copy-start.3
  24.0 0.8 copy-start.4
  24.8 0.8 copy-start.5
  25.5 0.8 copy-start.6
  27.0 0.7 copy-start.9
  36.9 9.8 %copy-start.12 = (s32[8]{0:T(128)S(1)}, s32[8]{0:T(128)}, u32[]{:S(2)}) copy-start(s32[8]{0:T(128)} %param.14) | copy-start | bytes 100
  36.9 9.9 %copy-start.10 = (f32[2,64]{1,0:T(2,128)S(1)}, f32[2,64]{1,0:T(2,128)}, u32[]{:S(2)}) copy-start(f32[2,64]{1,0:T(2,128)} %param.23) | copy-start | bytes 1540
  36.9 9.9 %copy-start.11 = (f32[2,64]{1,0:T(2,128)S(1)}, f32[2,64]{1,0:T(2,128)}, u32[]{:S(2)}) copy-start(f32[2,64]{1,0:T(2,128)} %param.24) | copy-start | bytes 1540
  36.9 25.0 %all-to-all-start.1 = ((f32[32,8,385]{2,1,0:T(8,128)}), f32[32,8,385]{2,1,0:T(8,128)S(1)}, u32[]{:S(2)}, u32[]{:S(2)}) async-start(f32[32,8,385]{2,1,0:T(8,128)} %pad_maximum_fusion), calls=%async_computation.1 | async-start | bytes 1048576 | tf_op jit(solution)/shard_map/all_to_all | solution.py:41
  46.8 15.7 %copy-start = (f32[2,8,1,64,64]{4,3,2,1,0:T(8,128)S(1)}, f32[2,8,1,64,64]{4,3,2,1,0:T(8,128)}, u32[]{:S(2)}) copy-start(f32[2,8,1,64,64]{4,3,2,1,0:T(8,128)} %param.25) | copy-start | bytes 786436
  79.0 0.8 copy-start.7
  102.6 0.7 copy-start.8
  103.9 18.1 %all-to-all-start.4 = ((bf16[32,8,128]{2,1,0:T(8,128)(2,1)}), bf16[32,8,128]{2,1,0:T(8,128)(2,1)S(1)}, u32[]{:S(2)}, u32[]{:S(2)}) async-start(bf16[32,8,128]{2,1,0:T(8,128)(2,1)} %broadcast_in_dim.39), calls=%async_computation.4 | async-start | bytes 131072 | tf_op jit(solution)/shard_map/all_to_all | solution.py:25
  158.7 22.8 %all-to-all-start.7 = ((f32[32,8,128]{2,1,0:T(8,128)}), f32[32,8,128]{2,1,0:T(8,128)S(1)}, u32[]{:S(2)}, u32[]{:S(2)}) async-start(f32[32,8,128]{2,1,0:T(8,128)} %fusion.42), calls=%async_computation.7 | async-start | bytes 262144 | tf_op jit(solution)/shard_map/all_to_all | solution.py:41
where the time goes:
time: 183 us; the launch traced here: 182 us
  blocking collectives  70.4 us (38%)
  waiting for transfers between devices  50 us (27%)
  starting transfers between devices  42 us (23%)
  local copies, waits for them, and re-layouts  10.3 us (6%)
  other arithmetic  4.75 us (3%)
  matrix products  3.7 us (2%)
    all_to_all x2, blocking collectives, sum_at_owner(): pieces = lax.all_to_all(cut_along(array, dim, size), axis, 0, 0, tiled=True)  41 us
    all_to_all x2, waiting for transfers between devices, sum_at_owner(): pieces = lax.all_to_all(cut_along(array, dim, size), axis, 0, 0, tiled=True)  30.1 us
    all_to_all x2, blocking collectives, sent_to_all(): lax.all_to_all(jnp.broadcast_to(array[None], (size, *array.shape)), axis,...  29.4 us
    all_to_all x2, starting transfers between devices, sent_to_all(): lax.all_to_all(jnp.broadcast_to(array[None], (size, *array.shape)), axis,...  25.6 us
    all_to_all x2, waiting for transfers between devices, sent_to_all(): lax.all_to_all(jnp.broadcast_to(array[None], (size, *array.shape)), axis,...  19.9 us
    all_to_all x2, starting transfers between devices, sum_at_owner(): pieces = lax.all_to_all(cut_along(array, dim, size), axis, 0, 0, tiled=True)  16.4 us
    unnamed x42, local copies, waits for them, and re-layouts  7.49 us
  transfers between devices with their start and end apart: 4, of which 4 were waited for; matrix products, arithmetic and copies ran while one was open for 2% of the time, Pallas kernels for 0%

commit v1 on v0

v1 whole, which is shorter than its diff:
```python
import jax
import jax.numpy as jnp
from jax import lax
from jax.experimental import pallas as pl
from jax.experimental.pallas import tpu as pltpu
from jax.sharding import PartitionSpec as P

D = 4096
LAYERS = 2
POSITION = 2048
HEAD = 64
ROWS = 8

DECAY_SCALE = 0.6065306597126334
NORM_EPS = 1e-06
KEY_EPS = 1e-05
GROUP_EPS = 0.00064

TP = 32
YS = 8
XS = 4

BF16 = jnp.bfloat16
F32 = jnp.float32


def sigmoid(v):
    return 1.0 / (1.0 + jnp.exp(-v))


def kernel(
    tok_hbm,
    len_smem,
    gain_hbm,
    wr_hbm,
    wk_hbm,
    wv_hbm,
    wd_hbm,
    wa_hbm,
    wg_hbm,
    wo_hbm,
    base_hbm,
    mix_hbm,
    state_hbm,
    next_out,
    state_out,
    tok,
    gain,
    wstage,
    wall,
    wout,
    base,
    mixg,
    prev,
    kept,
    x0,
    x1,
    pb_send,
    pb_recv,
    mb_send,
    mb_recv,
    ob_send,
    sum_recv,
    fin_recv,
    own_new,
    resid,
    load_sem,
    state_sem,
    out_sem,
    send_sem,
    gather_sem,
    x_sem,
    p_sem,
    m_sem,
    d_sem,
    r_sem,
):
    t = lax.axis_index("tp")
    dp = lax.axis_index("dp")
    y = dp // XS
    x = lax.rem(dp, XS)
    home = lax.rem(t, XS)
    group = t // XS
    is_owner = home == x

    def dev(tt, yy, xx):
        return {"tp": tt, "dp": yy * XS + xx}

    def wrap(v, n):
        return lax.rem(v + n, n)

    small = [
        (tok_hbm, tok),
        (gain_hbm, gain.at[x]),
        (wr_hbm, wstage.at[0]),
        (wk_hbm, wstage.at[1]),
        (wv_hbm, wstage.at[2]),
        (wd_hbm, wstage.at[3]),
        (wa_hbm, wstage.at[4]),
        (wg_hbm, wstage.at[5]),
        (wo_hbm, wout.at[x]),
        (base_hbm, base),
        (mix_hbm, mixg),
    ]
    loads = [
        pltpu.make_async_copy(src, dst, load_sem.at[i])
        for i, (src, dst) in enumerate(small)
    ]
    for load in loads:
        load.start()
    state_load = pltpu.make_async_copy(state_hbm, prev, state_sem)
    state_load.start()

    barrier = pltpu.get_barrier_semaphore()

    def greet(i, _):
        tt = wrap(t + i, TP)

        @pl.when(jnp.logical_or(i != 0, jnp.logical_not(is_owner)))
        def _():
            pl.semaphore_signal(barrier, 1, device_id=dev(tt, y, home))

        a = lax.rem(group + i // XS, YS)
        xx = wrap(x + lax.rem(i, XS), XS)

        @pl.when(jnp.logical_or(i != 0, jnp.logical_not(is_owner)))
        def _():
            pl.semaphore_signal(barrier, 1, device_id=dev(a * XS + x, y, xx))

        return 0

    lax.fori_loop(0, TP, greet, 0)
    for i in range(1, XS):
        pl.semaphore_signal(barrier, 1, device_id=dev(t, y, wrap(x + i, XS)))
    for i in range(1, YS):
        pl.semaphore_signal(barrier, 1, device_id=dev(t, wrap(y + i, YS), x))

    for load in loads:
        load.wait()
    for layer in range(LAYERS):
        for pair in range(3):
            wall[layer, x, :, pair * 128 : pair * 128 + 128] = jnp.concatenate(
                [wstage[2 * pair, layer], wstage[2 * pair + 1, layer]], axis=1
            )

    own = jnp.where(is_owner, 1, 0)
    pl.semaphore_wait(barrier, 2 * (TP - own) + (XS - 1) + (YS - 1))

    slot = x * YS + group

    def send_tokens(i, _):
        tt = wrap(t + TP // 2 + i, TP)
        pltpu.make_async_remote_copy(
            tok, x0.at[slot], send_sem.at[0], x_sem.at[0], device_id=dev(tt, y, home)
        ).start()
        return 0

    def send_tokens_skip(i, _):
        @pl.when(i != TP // 2)
        def _():
            send_tokens(i, 0)

        return 0

    lax.fori_loop(0, TP, send_tokens_skip, 0)

    @pl.when(is_owner)
    def _():
        pltpu.make_async_copy(tok, x0.at[slot], x_sem.at[0]).start()

    @pl.when(jnp.logical_not(is_owner))
    def _():
        send_tokens(TP // 2, 0)

    for layer in range(LAYERS):
        for i in (2, 1, 3):
            to = dev(t, y, wrap(x + i, XS))
            pltpu.make_async_remote_copy(
                wall.at[layer, x], wall.at[layer, x], send_sem.at[1], gather_sem.at[layer], device_id=to
            ).start()
        if layer == 0:
            for i in (2, 1, 3):
                to = dev(t, y, wrap(x + i, XS))
                pltpu.make_async_remote_copy(
                    gain.at[x], gain.at[x], send_sem.at[2], gather_sem.at[2], device_id=to
                ).start()
                pltpu.make_async_remote_copy(
                    wout.at[x], wout.at[x], send_sem.at[3], gather_sem.at[3], device_id=to
                ).start()

    def arrived(ref, sem):
        pltpu.make_async_copy(ref, ref, sem).wait()

    rows = lax.broadcasted_iota(jnp.int32, (ROWS, HEAD), 0)
    held = jnp.zeros((ROWS, HEAD), jnp.int32)
    for b in range(ROWS):
        held = jnp.where(rows == b, len_smem[b], held)
    live_rows = held > POSITION
    eye = (
        lax.broadcasted_iota(jnp.int32, (HEAD, HEAD), 0)
        == lax.broadcasted_iota(jnp.int32, (HEAD, HEAD), 1)
    ).astype(F32)

    state_load.wait()

    for layer in range(LAYERS):
        if layer == 0:
            arrived(gain.at[0:3], gather_sem.at[2])
            arrived(x0, x_sem.at[0])
            blocks = [
                x0[f * YS : (f + 1) * YS].astype(F32).reshape(YS * ROWS, 128)
                for f in range(XS)
            ]
        else:
            arrived(x1, x_sem.at[1])
            blocks = [x1[:, f].astype(F32).reshape(YS * ROWS, 128) for f in range(XS)]
        total = blocks[0] * blocks[0]
        for f in range(1, XS):
            total = total + blocks[f] * blocks[f]
        squares = jnp.sum(total, axis=1, keepdims=True)
        scaled = jnp.concatenate(
            [
                (blocks[f] * gain[f, layer : layer + 1, :]).astype(BF16)
                for f in range(XS)
            ],
            axis=1,
        )
        arrived(wall.at[layer, 0:3], gather_sem.at[layer])
        weights = wall[layer].reshape(XS * 128, 6 * HEAD)
        partial = jnp.dot(scaled, weights, preferred_element_type=F32)
        coarse = squares.astype(BF16).astype(F32)
        fine = squares - coarse
        lanes = lax.broadcasted_iota(jnp.int32, (YS * ROWS, 128), 1)
        tail = jnp.where(lanes < HEAD, coarse, fine)
        pb_send[layer, :, :, 0 : 6 * HEAD] = partial.reshape(YS, ROWS, 6 * HEAD).astype(BF16)
        pb_send[layer, :, :, 6 * HEAD :] = tail.reshape(YS, ROWS, 128).astype(BF16)
        for i in (4, 3, 5, 2, 6, 1, 7):
            yy = wrap(y + i, YS)
            pltpu.make_async_remote_copy(
                pb_send.at[layer, yy],
                pb_recv.at[layer, y],
                send_sem.at[4 + layer],
                p_sem.at[layer],
                device_id=dev(t, yy, x),
            ).start()
        pb_recv[layer, y] = pb_send[layer, y]
        arrived(pb_recv.at[layer, 0:7], p_sem.at[layer])
        summed = pb_recv[layer, 0].astype(F32)
        for i in range(1, YS):
            summed = summed + pb_recv[layer, i].astype(F32)
        sq = summed[:, 6 * HEAD : 6 * HEAD + 1] + summed[:, 7 * HEAD : 7 * HEAD + 1]
        projected = summed * lax.rsqrt(sq / D + NORM_EPS)
        recept, key, value, decay_pre, rate_pre, gate_pre = [
            projected[:, j * HEAD : (j + 1) * HEAD] for j in range(6)
        ]
        decay = jnp.exp(-DECAY_SCALE * sigmoid(decay_pre + base[layer : layer + 1, :]))
        unit = key * lax.rsqrt(jnp.sum(key * key, axis=1, keepdims=True) + KEY_EPS)
        correction = unit * sigmoid(rate_pre)
        readouts = []
        for b in range(ROWS):
            one = slice(b, b + 1)
            state = prev[layer, b]
            removed = -jnp.sum(state * unit[one], axis=1, keepdims=True)
            value_col = jnp.sum(eye * value[one], axis=1, keepdims=True)
            updated = state * decay[one] + removed * correction[one] + value_col * key[one]
            read = jnp.sum(updated * recept[one], axis=1, keepdims=True)
            readouts.append(jnp.sum(eye * read, axis=0, keepdims=True))
            alive = jnp.full((HEAD, HEAD), len_smem[b], jnp.int32) > POSITION
            kept[layer, b] = jnp.where(alive, updated, state)
        pltpu.make_async_copy(kept.at[layer], state_out.at[layer], out_sem.at[layer]).start()
        readout = jnp.concatenate(readouts, axis=0)
        centre = jnp.sum(readout, axis=1, keepdims=True) / HEAD
        off = readout - centre
        spread = jnp.sum(off * off, axis=1, keepdims=True) / HEAD
        normed = off * lax.rsqrt(spread + GROUP_EPS)
        normed = normed * mixg[layer : layer + 1, :] * sigmoid(gate_pre)
        mixed = jnp.where(live_rows, normed, 0.0)
        mb_send[layer] = jnp.concatenate([mixed, mixed], axis=1).astype(BF16)
        for i in (4, 3, 5, 2, 6, 1, 7):
            yy = wrap(y + i, YS)
            pltpu.make_async_remote_copy(
                mb_send.at[layer],
                mb_recv.at[layer, y],
                send_sem.at[6 + layer],
                m_sem.at[layer],
                device_id=dev(t, yy, x),
            ).start()
        mb_recv[layer, y] = mb_send[layer]
        if layer == 0:
            arrived(wout.at[0:3], gather_sem.at[3])
        arrived(mb_recv.at[layer, 0:7], m_sem.at[layer])
        everyone = mb_recv[layer].astype(F32).reshape(YS * ROWS, 128)[:, :HEAD].astype(BF16)
        for f in range(XS):
            term = jnp.dot(everyone, wout[f, layer], preferred_element_type=F32)
            ob_send[layer, :, f] = term.reshape(YS, ROWS, 128).astype(BF16)

        if layer == 0:
            def send_sums(i, _):
                a = wrap(group + YS // 2 + i, YS)

                @pl.when(jnp.logical_or(i != YS // 2, jnp.logical_not(is_owner)))
                def _():
                    pltpu.make_async_remote_copy(
                        ob_send.at[0, a],
                        sum_recv.at[t],
                        send_sem.at[8],
                        d_sem.at[0],
                        device_id=dev(a * XS + x, y, x),
                    ).start()

                return 0

            lax.fori_loop(0, YS, send_sums, 0)

            @pl.when(is_owner)
            def _():
                sum_recv[t] = ob_send[0, group]
                arrived(sum_recv.at[0 : TP - 1], d_sem.at[0])
                acc = sum_recv[0].astype(F32)
                for i in range(1, TP):
                    acc = acc + sum_recv[i].astype(F32)
                for f in range(XS):
                    own_new[f] = (x0[f * YS + group].astype(F32) + acc[f]).astype(BF16)

                def send_new(i, _):
                    tt = wrap(t + TP // 2 + i, TP)

                    @pl.when(i != TP // 2)
                    def _():
                        pltpu.make_async_remote_copy(
                            own_new,
                            x1.at[group],
                            send_sem.at[9],
                            x_sem.at[1],
                            device_id=dev(tt, y, x),
                        ).start()

                    return 0

                lax.fori_loop(0, TP, send_new, 0)
                pltpu.make_async_copy(own_new, x1.at[group], x_sem.at[1]).start()
                for i in range(1, XS):
                    xx = wrap(x + i, XS)
                    pltpu.make_async_remote_copy(
                        own_new.at[xx],
                        resid,
                        send_sem.at[10],
                        r_sem,
                        device_id=dev(t, y, xx),
                    ).start()
                pltpu.make_async_copy(own_new.at[x], resid, r_sem).start()

        else:
            def send_last(i, _):
                a = wrap(group + YS // 2 + i // XS, YS)
                xx = wrap(x + lax.rem(i, XS), XS)

                @pl.when(jnp.logical_or(i != TP // 2, jnp.logical_not(is_owner)))
                def _():
                    pltpu.make_async_remote_copy(
                        ob_send.at[1, a, xx],
                        fin_recv.at[t],
                        send_sem.at[11],
                        d_sem.at[1],
                        device_id=dev(a * XS + x, y, xx),
                    ).start()

                return 0

            lax.fori_loop(0, TP, send_last, 0)

            @pl.when(is_owner)
            def _():
                pltpu.make_async_copy(
                    ob_send.at[1, group, x], fin_recv.at[t], d_sem.at[1]
                ).start()

            arrived(resid, r_sem)
            arrived(fin_recv, d_sem.at[1])
            acc = fin_recv[0].astype(F32)
            for i in range(1, TP):
                acc = acc + fin_recv[i].astype(F32)
            next_out[...] = (resid[...].astype(F32) + acc).astype(BF16)

    arrived(x0.at[0 : TP - 1], send_sem.at[0])

    @pl.when(jnp.logical_not(is_owner))
    def _():
        arrived(x0.at[0], send_sem.at[0])
        arrived(ob_send.at[0, 0], send_sem.at[8])
        arrived(fin_recv.at[0], send_sem.at[11])

    @pl.when(is_owner)
    def _():
        arrived(sum_recv.at[0 : TP - 1], send_sem.at[9])
        arrived(own_new.at[0:3], send_sem.at[10])

    for layer in range(LAYERS):
        arrived(wall.at[layer, 0:3], send_sem.at[1])
        arrived(pb_recv.at[layer, 0:7], send_sem.at[4 + layer])
        arrived(mb_recv.at[layer, 0:7], send_sem.at[6 + layer])
        pltpu.make_async_copy(kept.at[layer], state_out.at[layer], out_sem.at[layer]).wait()
    arrived(gain.at[0:3], send_sem.at[2])
    arrived(wout.at[0:3], send_sem.at[3])
    arrived(ob_send.at[0, 0:7], send_sem.at[8])
    arrived(fin_recv.at[0 : TP - 1], send_sem.at[11])


def on_device(
    tokens,
    lengths,
    in_gain,
    w_recept,
    w_key,
    w_value,
    w_decay,
    w_rate,
    w_gate,
    w_out,
    decay_base,
    mix_gain,
    states,
):
    hbm = pl.BlockSpec(memory_space=pl.ANY)
    vmem = pltpu.VMEM
    dma = pltpu.SemaphoreType.DMA
    squeezed = states.reshape(LAYERS, ROWS, HEAD, HEAD)
    next_tokens, new_states = pl.pallas_call(
        kernel,
        out_shape=(
            jax.ShapeDtypeStruct(tokens.shape, BF16),
            jax.ShapeDtypeStruct(squeezed.shape, F32),
        ),
        in_specs=[hbm, pl.BlockSpec(memory_space=pltpu.SMEM)] + [hbm] * 11,
        out_specs=(pl.BlockSpec(memory_space=pltpu.VMEM), hbm),
        scratch_shapes=[
            vmem((ROWS, 128), BF16),
            vmem((XS, LAYERS, 128), F32),
            vmem((6, LAYERS, 128, HEAD), BF16),
            vmem((LAYERS, XS, 128, 6 * HEAD), BF16),
            vmem((XS, LAYERS, HEAD, 128), BF16),
            vmem((LAYERS, HEAD), F32),
            vmem((LAYERS, HEAD), F32),
            vmem((LAYERS, ROWS, HEAD, HEAD), F32),
            vmem((LAYERS, ROWS, HEAD, HEAD), F32),
            vmem((XS * YS, ROWS, 128), BF16),
            vmem((YS, XS, ROWS, 128), BF16),
            vmem((LAYERS, YS, ROWS, 512), BF16),
            vmem((LAYERS, YS, ROWS, 512), BF16),
            vmem((LAYERS, ROWS, 128), BF16),
            vmem((LAYERS, YS, ROWS, 128), BF16),
            vmem((LAYERS, YS, XS, ROWS, 128), BF16),
            vmem((TP, XS, ROWS, 128), BF16),
            vmem((TP, ROWS, 128), BF16),
            vmem((XS, ROWS, 128), BF16),
            vmem((ROWS, 128), BF16),
            dma((11,)),
            dma(()),
            dma((LAYERS,)),
            dma((12,)),
            dma((4,)),
            dma((2,)),
            dma((LAYERS,)),
            dma((LAYERS,)),
            dma((2,)),
            dma(()),
        ],
        compiler_params=pltpu.CompilerParams(collective_id=0, has_side_effects=True),
        name="decode_step",
    )(
        tokens,
        lengths,
        in_gain,
        w_recept,
        w_key,
        w_value,
        w_decay,
        w_rate,
        w_gate,
        w_out,
        decay_base,
        mix_gain,
        squeezed,
    )
    return (next_tokens, new_states.reshape(states.shape))


def solution(mesh):
    in_specs = (
        P("tp", "dp"),
        P("dp"),
        P(None, "dp"),
        P(None, "dp", "tp"),
        P(None, "dp", "tp"),
        P(None, "dp", "tp"),
        P(None, "dp", "tp"),
        P(None, "dp", "tp"),
        P(None, "dp", "tp"),
        P(None, "tp", "dp"),
        P(None, "tp"),
        P(None, "tp"),
        P(None, "dp", "tp", None, None),
    )
    out_specs = (P("tp", "dp"), P(None, "dp", "tp", None, None))
    return jax.shard_map(
        on_device, mesh=mesh, in_specs=in_specs, out_specs=out_specs, check_vma=False
    )
```

time: 183 us -> 90.2 us (0.49)
  Pallas kernels: 0 us -> 80 us
  blocking collectives: 70.4 us -> 0 us
  waiting for transfers between devices: 50 us -> 0 us
  starting transfers between devices: 42 us -> 0 us
  other arithmetic: 4.75 us -> 0 us
  matrix products: 3.7 us -> 0 us
  local copies, waits for them, and re-layouts: 10.3 us -> 8.37 us
    pallas_call x0 -> x1, Pallas kernels: none -> 80 us  [on_device(): pl.pallas_call(kernel, out_shape=(jax.ShapeDtypeStruct(tokens.shape, BF16...]
    all_to_all x4 -> x0, blocking collectives: 70.4 us -> none  [the longest x2 41 us: sum_at_owner(): pieces = lax.all_to_all(cut_along(array, dim, size), axis, 0, 0, tiled=True)]
    all_to_all x4 -> x0, waiting for transfers between devices: 50 us -> none  [the longest x2 30.1 us: sum_at_owner(): pieces = lax.all_to_all(cut_along(array, dim, size), axis, 0, 0, tiled=True)]
    all_to_all x4 -> x0, starting transfers between devices: 42 us -> none  [the longest x2 25.6 us: sent_to_all(): lax.all_to_all(jnp.broadcast_to(array[None], (size, *array.shape)), axis,...]
    dot_general x8 -> x0, matrix products: 3.7 us -> none  [the longest x2 1.33 us: update_heads(): jnp.einsum('bhvk,bhk->bhv', updated, recept_heads, precision=lax.Precisio...]
    broadcast_in_dim x4 -> x0, local copies, waits for them, and re-layouts: 2.02 us -> none  [sent_to_all(): jnp.broadcast_to(array[None], (size, *array.shape))]
    unnamed x42 -> x20, local copies, waits for them, and re-layouts: 7.49 us -> 8.37 us
  transfers between devices with their start and end apart: 4 -> 0, of which waited for: 4 -> 0; matrix products, arithmetic and copies ran while one was open for 2% -> 0% of each run, Pallas kernels for 0% -> 0%
where the time goes in v1:
time: 90.2 us; the launch traced here: 89.1 us
  Pallas kernels  80 us (89%)
  local copies, waits for them, and re-layouts  8.37 us (9%)
    pallas_call x1, Pallas kernels, on_device(): pl.pallas_call(kernel, out_shape=(jax.ShapeDtypeStruct(tokens.shape, BF16...  80 us
    unnamed x20, local copies, waits for them, and re-layouts  8.37 us

profile of v1, /device:TPU:1, one launch (start us, length us, event | category | flops | bytes accessed | tf_op | source)
XLA Modules:
  0.0 89.1 jit_solution(18018050433292080572)
XLA Ops:
  0.6 0.0 copy-start
  0.6 1.5 %copy.15.wr_hbm = bf16[2,128,64]{2,1,0:T(8,128)(2,1)} copy(bf16[2,128,64]{1,2,0:T(8,128)(2,1)} %param.16) | data formatting | bytes 65536 | tf_op args[3]
  2.1 0.0 copy-done
  2.1 0.0 copy-start.1
  2.1 0.7 copy.16.wk_hbm
  2.9 0.0 copy-done.1
  2.9 0.0 copy-start.2
  2.9 0.7 copy.17.wv_hbm
  3.6 0.0 copy-done.2
  3.7 0.0 copy-start.3
  3.7 0.7 copy.18.wd_hbm
  4.4 0.0 copy-done.3
  4.4 0.0 copy-start.4
  4.4 0.7 copy.19.wa_hbm
  5.2 0.0 copy-done.4
  5.2 0.7 copy.20.wg_hbm
  5.9 80.0 %decode_step.1 = (bf16[8,128]{1,0:T(8,128)(2,1)}, f32[2,8,64,64]{3,2,1,0:T(8,128)}) custom-call(bf16[8,128]{1,0:T(8,128)(2,1)} %tok_hbm.1, s32[8]{0:T(128)} %len_smem.1, f32[2,128]{1,0:T(2,128)} %gain_hbm.1, bf16[2,128,64]{2,1,0:T(8,128)(2,1)} %copy.15.wr_hbm, bf16[2,128,64]{2,1,0:T(8,128)(2,1)} %copy.16.wk_hbm, bf16[2,128,64]{2,1,0:T(8,128)(2,1)} %copy.17.wv_hbm, ...), custom_call_target="tpu_custom_call" | custom-call | tf_op jit(solution)/shard_map/decode_step/pallas_call | solution.py:428
  85.9 0.0 copy-start.5
  86.0 0.6 copy-done.5
  86.6 0.6 copy.24
  87.2 1.9 %copy.25 = f32[2,8,1,64,64]{4,3,2,1,0:T(8,128)} copy(f32[2,8,1,64,64]{4,3,2,1,0:T(8,128)} %bitcast.5) | data formatting | bytes 524288
Async XLA Ops:
  0.6 1.5 %copy-start = (bf16[2,128,64]{1,2,0:T(8,128)(2,1)S(1)}, bf16[2,128,64]{1,2,0:T(8,128)(2,1)}, u32[]{:S(2)}) copy-start(bf16[2,128,64]{1,2,0:T(8,128)(2,1)} %param.17) | copy-start | bytes 98308
  2.1 0.8 copy-start.1
  2.9 0.8 copy-start.2
  3.7 0.8 copy-start.3
  4.4 0.8 copy-start.4
  85.9 0.7 copy-start.5

commit v2 on v1

--- a/solution.py
+++ b/solution.py
@@ -46,13 +46,11 @@
     state_out,
     tok,
     gain,
-    wstage,
     wall,
     wout,
     base,
     mixg,
     prev,
-    kept,
     x0,
     x1,
     pb_send,
@@ -66,7 +64,6 @@
     resid,
     load_sem,
     state_sem,
-    out_sem,
     send_sem,
     gather_sem,
     x_sem,
@@ -89,22 +86,21 @@
     def wrap(v, n):
         return lax.rem(v + n, n)
 
-    small = [
-        (tok_hbm, tok),
+    token_load = pltpu.make_async_copy(tok_hbm, tok, load_sem.at[0])
+    token_load.start()
+    loads = []
+    for layer in range(LAYERS):
+        for j, ref in enumerate((wr_hbm, wk_hbm, wv_hbm, wd_hbm, wa_hbm, wg_hbm)):
+            loads.append((ref.at[layer], wall.at[layer, x, j * HEAD : (j + 1) * HEAD]))
+    loads += [
         (gain_hbm, gain.at[x]),
-        (wr_hbm, wstage.at[0]),
-        (wk_hbm, wstage.at[1]),
-        (wv_hbm, wstage.at[2]),
-        (wd_hbm, wstage.at[3]),
-        (wa_hbm, wstage.at[4]),
-        (wg_hbm, wstage.at[5]),
         (wo_hbm, wout.at[x]),
         (base_hbm, base),
         (mix_hbm, mixg),
     ]
     loads = [
-        pltpu.make_async_copy(src, dst, load_sem.at[i])
-        for i, (src, dst) in enumerate(small)
+        pltpu.make_async_copy(src, dst, load_sem.at[1 + i])
+        for i, (src, dst) in enumerate(loads)
     ]
     for load in loads:
         load.start()
@@ -113,35 +109,39 @@
 
     barrier = pltpu.get_barrier_semaphore()
 
+    def ring(i):
+        step = (i + 1) // 2
+        return TP // 2 + jnp.where(lax.rem(i, 2) == 1, step, -step)
+
     def greet(i, _):
-        tt = wrap(t + i, TP)
-
-        @pl.when(jnp.logical_or(i != 0, jnp.logical_not(is_owner)))
-        def _():
-            pl.semaphore_signal(barrier, 1, device_id=dev(tt, y, home))
-
-        a = lax.rem(group + i // XS, YS)
+        tt = wrap(t + ring(i), TP)
+        pl.semaphore_signal(barrier, 1, device_id=dev(tt, y, home))
+        return 0
+
+    lax.fori_loop(0, TP - 1, greet, 0)
+
+    def greet_back(i, _):
+        a = wrap(group + YS // 2 + i // XS, YS)
         xx = wrap(x + lax.rem(i, XS), XS)
 
-        @pl.when(jnp.logical_or(i != 0, jnp.logical_not(is_owner)))
+        @pl.when(jnp.logical_or(i != TP // 2, jnp.logical_not(is_owner)))
         def _():
             pl.semaphore_signal(barrier, 1, device_id=dev(a * XS + x, y, xx))
 
         return 0
 
-    lax.fori_loop(0, TP, greet, 0)
+    lax.fori_loop(0, TP, greet_back, 0)
+
+    @pl.when(jnp.logical_not(is_owner))
+    def _():
+        pl.semaphore_signal(barrier, 1, device_id=dev(t, y, home))
+
     for i in range(1, XS):
         pl.semaphore_signal(barrier, 1, device_id=dev(t, y, wrap(x + i, XS)))
     for i in range(1, YS):
         pl.semaphore_signal(barrier, 1, device_id=dev(t, wrap(y + i, YS), x))
 
-    for load in loads:
-        load.wait()
-    for layer in range(LAYERS):
-        for pair in range(3):
-            wall[layer, x, :, pair * 128 : pair * 128 + 128] = jnp.concatenate(
-                [wstage[2 * pair, layer], wstage[2 * pair + 1, layer]], axis=1
-            )
+    token_load.wait()
 
     own = jnp.where(is_owner, 1, 0)
     pl.semaphore_wait(barrier, 2 * (TP - own) + (XS - 1) + (YS - 1))
@@ -149,20 +149,13 @@
     slot = x * YS + group
 
     def send_tokens(i, _):
-        tt = wrap(t + TP // 2 + i, TP)
+        tt = wrap(t + ring(i), TP)
         pltpu.make_async_remote_copy(
             tok, x0.at[slot], send_sem.at[0], x_sem.at[0], device_id=dev(tt, y, home)
         ).start()
         return 0
 
-    def send_tokens_skip(i, _):
-        @pl.when(i != TP // 2)
-        def _():
-            send_tokens(i, 0)
-
-        return 0
-
-    lax.fori_loop(0, TP, send_tokens_skip, 0)
+    lax.fori_loop(0, TP - 1, send_tokens, 0)
 
     @pl.when(is_owner)
     def _():
@@ -170,7 +163,10 @@
 
     @pl.when(jnp.logical_not(is_owner))
     def _():
-        send_tokens(TP // 2, 0)
+        send_tokens(TP - 1, 0)
+
+    for load in loads:
+        load.wait()
 
     for layer in range(LAYERS):
         for i in (2, 1, 3):
@@ -218,16 +214,16 @@
         for f in range(1, XS):
             total = total + blocks[f] * blocks[f]
         squares = jnp.sum(total, axis=1, keepdims=True)
-        scaled = jnp.concatenate(
-            [
-                (blocks[f] * gain[f, layer : layer + 1, :]).astype(BF16)
-                for f in range(XS)
-            ],
-            axis=1,
-        )
         arrived(wall.at[layer, 0:3], gather_sem.at[layer])
-        weights = wall[layer].reshape(XS * 128, 6 * HEAD)
-        partial = jnp.dot(scaled, weights, preferred_element_type=F32)
+        partial = None
+        for f in range(XS):
+            term = lax.dot_general(
+                (blocks[f] * gain[f, layer : layer + 1, :]).astype(BF16),
+                wall[layer, f],
+                (((1,), (1,)), ((), ())),
+                preferred_element_type=F32,
+            )
+            partial = term if partial is None else partial + term
         coarse = squares.astype(BF16).astype(F32)
         fine = squares - coarse
         lanes = lax.broadcasted_iota(jnp.int32, (YS * ROWS, 128), 1)
@@ -256,19 +252,20 @@
         decay = jnp.exp(-DECAY_SCALE * sigmoid(decay_pre + base[layer : layer + 1, :]))
         unit = key * lax.rsqrt(jnp.sum(key * key, axis=1, keepdims=True) + KEY_EPS)
         correction = unit * sigmoid(rate_pre)
-        readouts = []
+        read_key = decay * recept
+        read_fix = jnp.sum(correction * recept, axis=1, keepdims=True)
+        read_value = jnp.sum(key * recept, axis=1, keepdims=True)
+        removals = []
+        reads = []
         for b in range(ROWS):
             one = slice(b, b + 1)
             state = prev[layer, b]
             removed = -jnp.sum(state * unit[one], axis=1, keepdims=True)
-            value_col = jnp.sum(eye * value[one], axis=1, keepdims=True)
-            updated = state * decay[one] + removed * correction[one] + value_col * key[one]
-            read = jnp.sum(updated * recept[one], axis=1, keepdims=True)
-            readouts.append(jnp.sum(eye * read, axis=0, keepdims=True))
-            alive = jnp.full((HEAD, HEAD), len_smem[b], jnp.int32) > POSITION
-            kept[layer, b] = jnp.where(alive, updated, state)
-        pltpu.make_async_copy(kept.at[layer], state_out.at[layer], out_sem.at[layer]).start()
-        readout = jnp.concatenate(readouts, axis=0)
+            read = jnp.sum(state * read_key[one], axis=1, keepdims=True)
+            removals.append(removed)
+            read = read + removed * read_fix[one]
+            reads.append(jnp.sum(eye * read, axis=0, keepdims=True))
+        readout = jnp.concatenate(reads, axis=0) + value * read_value
         centre = jnp.sum(readout, axis=1, keepdims=True) / HEAD
         off = readout - centre
         spread = jnp.sum(off * off, axis=1, keepdims=True) / HEAD
@@ -286,6 +283,15 @@
                 device_id=dev(t, yy, x),
             ).start()
         mb_recv[layer, y] = mb_send[layer]
+        for b in range(ROWS):
+            one = slice(b, b + 1)
+            state = prev[layer, b]
+            value_col = jnp.sum(eye * value[one], axis=1, keepdims=True)
+            updated = (
+                state * decay[one] + removals[b] * correction[one] + value_col * key[one]
+            )
+            alive = jnp.full((HEAD, HEAD), len_smem[b], jnp.int32) > POSITION
+            state_out[layer, b] = jnp.where(alive, updated, state)
         if layer == 0:
             arrived(wout.at[0:3], gather_sem.at[3])
         arrived(mb_recv.at[layer, 0:7], m_sem.at[layer])
@@ -399,7 +405,6 @@
         arrived(wall.at[layer, 0:3], send_sem.at[1])
         arrived(pb_recv.at[layer, 0:7], send_sem.at[4 + layer])
         arrived(mb_recv.at[layer, 0:7], send_sem.at[6 + layer])
-        pltpu.make_async_copy(kept.at[layer], state_out.at[layer], out_sem.at[layer]).wait()
     arrived(gain.at[0:3], send_sem.at[2])
     arrived(wout.at[0:3], send_sem.at[3])
     arrived(ob_send.at[0, 0:7], send_sem.at[8])
@@ -424,24 +429,26 @@
     hbm = pl.BlockSpec(memory_space=pl.ANY)
     vmem = pltpu.VMEM
     dma = pltpu.SemaphoreType.DMA
+    turned = [
+        jnp.swapaxes(w, 1, 2)
+        for w in (w_recept, w_key, w_value, w_decay, w_rate, w_gate)
+    ]
     squeezed = states.reshape(LAYERS, ROWS, HEAD, HEAD)
     next_tokens, new_states = pl.pallas_call(
         kernel,
         out_shape=(
-            jax.ShapeDtypeStruct(tokens.shape, BF16),
-            jax.ShapeDtypeStruct(squeezed.shape, F32),
+            pltpu.VMEM(tokens.shape, BF16),
+            pltpu.VMEM(squeezed.shape, F32),
         ),
         in_specs=[hbm, pl.BlockSpec(memory_space=pltpu.SMEM)] + [hbm] * 11,
-        out_specs=(pl.BlockSpec(memory_space=pltpu.VMEM), hbm),
+        out_specs=(pl.BlockSpec(memory_space=pltpu.VMEM), pl.BlockSpec(memory_space=pltpu.VMEM)),
         scratch_shapes=[
             vmem((ROWS, 128), BF16),
             vmem((XS, LAYERS, 128), F32),
-            vmem((6, LAYERS, 128, HEAD), BF16),
-            vmem((LAYERS, XS, 128, 6 * HEAD), BF16),
+            vmem((LAYERS, XS, 6 * HEAD, 128), BF16),
             vmem((XS, LAYERS, HEAD, 128), BF16),
             vmem((LAYERS, HEAD), F32),
             vmem((LAYERS, HEAD), F32),
-            vmem((LAYERS, ROWS, HEAD, HEAD), F32),
             vmem((LAYERS, ROWS, HEAD, HEAD), F32),
             vmem((XS * YS, ROWS, 128), BF16),
             vmem((YS, XS, ROWS, 128), BF16),
@@ -454,9 +461,8 @@
             vmem((TP, ROWS, 128), BF16),
             vmem((XS, ROWS, 128), BF16),
             vmem((ROWS, 128), BF16),
-            dma((11,)),
+            dma((17,)),
             dma(()),
-            dma((LAYERS,)),
             dma((12,)),
             dma((4,)),
             dma((2,)),
@@ -471,12 +477,7 @@
         tokens,
         lengths,
         in_gain,
-        w_recept,
-        w_key,
-        w_value,
-        w_decay,
-        w_rate,
-        w_gate,
+        *turned,
         w_out,
         decay_base,
         mix_gain,

time: 90.2 us -> 81.6 us (0.905); the launches traced: 89.1 us -> 81.5 us
  local copies, waits for them, and re-layouts: 8.37 us -> 1.37 us
    unnamed x20 -> x2, local copies, waits for them, and re-layouts: 8.37 us -> 1.37 us
where the time goes in v2:
time: 81.6 us; the launch traced here: 81.5 us
  Pallas kernels  79.5 us (97%)
  local copies, waits for them, and re-layouts  1.37 us (2%)
    pallas_call x1, Pallas kernels, on_device(): pl.pallas_call(kernel, out_shape=(pltpu.VMEM(tokens.shape, BF16), pltpu.V...  79.5 us

profile of v2, /device:TPU:1, one launch (start us, length us, event | category | flops | bytes accessed | tf_op | source)
XLA Modules:
  0.0 81.5 jit_solution(9138720878217670629)
XLA Ops:
  0.6 79.5 %decode_step.1 = (bf16[8,128]{1,0:T(8,128)(2,1)S(1)}, f32[2,8,64,64]{3,2,1,0:T(8,128)S(1)}) custom-call(bf16[8,128]{1,0:T(8,128)(2,1)} %tok_hbm.1, s32[8]{0:T(128)} %len_smem.1, f32[2,128]{1,0:T(2,128)} %gain_hbm.1, bf16[2,64,128]{2,1,0:T(8,128)(2,1)} %bitcast.12, bf16[2,64,128]{2,1,0:T(8,128)(2,1)} %bitcast.13, bf16[2,64,128]{2,1,0:T(8,128)(2,1)} %bitcast.14, ...), custom_call_target="tpu_custom_call" | custom-call | tf_op jit(solution)/shard_map/decode_step/pallas_call | solution.py:437
  80.1 0.6 copy.18
  80.7 0.8 copy.19
